TPU v7x, 32 devices: a whole 2x2x4 slice. The times are simulated.
32 devices in a mesh: ep: 8 (over z, y), tp: 4 (over x, core).
Axes of the slice: x: 2, y: 2, z: 4, core: 2. Of those that a mesh axis runs over, the one named last changes fastest.
Arguments:
- tokens: bfloat16 [2048, 2048], P('ep', 'tp'), may hold values from -72 to 72
- norm_gain: bfloat16 [2048], P('tp'), may hold values from 0.099609375 to 1.8984375
- expert_ids: int32 [2048, 2], P('ep'), may hold values from 0 to 7, all different within a row; in each aligned block of 256 rows (0 to 255, 256 to 511, ...) at most 128 rows name the same one
- gate_share: float32 [2048, 2], P('ep'), may hold values from 0.1 to 1
- gate_weight: bfloat16 [8, 2048, 4096], P('ep', None, 'tp'), may hold values from -0.125 to 0.125
- up_weight: bfloat16 [8, 2048, 4096], P('ep', None, 'tp'), may hold values from -0.125 to 0.125
- down_weight: bfloat16 [8, 4096, 2048], P('ep', 'tp'), may hold values from -0.09375 to 0.09375
Outputs:
- mixed: bfloat16 [2048, 2048], P('ep', 'tp')
Inputs may be any that keep to these rules, and one draw needn't show every extreme that they name: `expert_ids`: each token names two different experts; among the 256 tokens of one index of ep no expert is named more than 128 times, a bound that some block reaches.
All inputs are finite; a program needn't handle non-finite values.
Results may differ from a plain program's by a relative error of at most 0.019.
Values may be sent and summed in bfloat16 or wider, within the bound.
A program may use at most 64 MiB of HBM per device.

v0:
```python
import functools
import jax
import jax.numpy as jnp
from jax import lax
from jax.experimental import pallas as pl
from jax.experimental.pallas import tpu as pltpu
from jax.sharding import PartitionSpec as P

D = 2048


EPS = 1e-06
MESH = pl.DeviceIdType.MESH
BF = jnp.bfloat16
F32 = jnp.float32
CORES = 2


def plain(tokens, norm_gain, expert_ids, gate_share, gate_weight, up_weight, down_weight):
    n_expdev = lax.axis_size("ep")
    exp_local = gate_weight.shape[0]
    experts = exp_local * n_expdev
    tok_rows = tokens.shape[0]
    slot_cap = 4 * tok_rows // experts
    flat_ids = expert_ids.reshape(-1)
    onehot = (flat_ids[:, None] == jnp.arange(experts, dtype=jnp.int32)[None, :]).astype(jnp.int32)
    slots = jnp.sum((jnp.cumsum(onehot, axis=0) - onehot) * onehot, axis=1)
    target = flat_ids * slot_cap + slots
    values = tokens.astype(jnp.float32)
    squares = lax.psum(jnp.sum(values * values, axis=1), "tp")
    factor = lax.rsqrt(squares / D + EPS)
    normed = (values * factor[:, None] * norm_gain.astype(jnp.float32)[None, :]).astype(
        jnp.bfloat16
    )
    rows = jnp.repeat(normed, 2, axis=0)
    buffer = jnp.zeros((experts * slot_cap, normed.shape[1]), jnp.bfloat16).at[target].set(rows)
    buffer = buffer.reshape(n_expdev, exp_local, slot_cap, normed.shape[1])
    arrived = lax.all_to_all(buffer, "ep", split_axis=0, concat_axis=0, tiled=True)
    piece = lax.all_gather(arrived, "tp", axis=3, tiled=True)
    first = jnp.einsum("secd,edf->secf", piece, gate_weight, preferred_element_type=jnp.float32)
    second = jnp.einsum("secd,edf->secf", piece, up_weight, preferred_element_type=jnp.float32)
    hidden = (jax.nn.silu(first) * second).astype(jnp.bfloat16)
    width_local = D // lax.axis_size("tp")
    term = jnp.einsum("secf,efd->dsec", hidden, down_weight, preferred_element_type=jnp.float32)
    summed = lax.psum_scatter(
        term.reshape(lax.axis_size("tp") * width_local, n_expdev * exp_local * slot_cap).astype(
            jnp.bfloat16
        ),
        "tp",
        scatter_dimension=0,
        tiled=True,
    )
    results = summed.reshape(width_local, n_expdev, exp_local, slot_cap)
    results = jnp.transpose(results, (1, 2, 3, 0))
    returned = lax.all_to_all(results, "ep", split_axis=0, concat_axis=0, tiled=True)
    flat_back = returned.reshape(experts * slot_cap, width_local)
    picked = flat_back[target].astype(jnp.float32).reshape(tok_rows, 2, width_local)
    return jnp.sum(picked * gate_share[:, :, None], axis=1).astype(jnp.bfloat16)


def fused(
    n, n_tp, steps,
    tok_ref, gain_ref, ids_ref, share_ref, wg_hbm, wu_hbm, wd_hbm,
    out_ref,
    wg, wu, wd, part, near, far, slot_row, share_row, send_a, send_b, xs,
    hid, own_y, ys, yd, za, zs, zx, rs, ra, mix_hi, mix_lo,
    w_sem, p_send, p_recv, n_send, n_recv, a_send, a_recv, b_send, b_recv,
    f_send, f_recv, d_send, d_recv, e_send, e_recv, y_send, y_recv, z_send, z_recv, r_send, r_recv,
):
    me = lax.axis_index("ep")
    tp = lax.axis_index("tp")
    x, c = tp // CORES, tp % CORES
    partner = x * CORES + (1 - c)
    across = (1 - x) * CORES + c
    diag = (1 - x) * CORES + (1 - c)
    rows, width = tok_ref.shape
    cap = send_a.shape[1]
    half = n // 2

    def peer(k):
        found, bit = 0, 1
        while bit < n:
            found = found + (me // bit + k // bit) % 2 * bit
            bit *= 2
        return found

    loads = [
        pltpu.make_async_copy(wg_hbm.at[0], wg, w_sem.at[0]),
        pltpu.make_async_copy(wu_hbm.at[0], wu, w_sem.at[1]),
    ] + [
        pltpu.make_async_copy(wd_hbm.at[0, :, pl.ds(q * width, width)], wd.at[q], w_sem.at[2 + q])
        for q in range(n_tp)
    ]
    for load in loads:
        load.start()

    barrier = pltpu.get_barrier_semaphore()
    for other in (partner, across, diag):
        pl.semaphore_signal(barrier, inc=1, device_id=(me, other), device_id_type=MESH)
    for k in range(1, n):
        pl.semaphore_signal(barrier, inc=1, device_id=(peer(k), tp), device_id_type=MESH)

    def remote(src, dst, ssem, rsem, e, t):
        return pltpu.make_async_remote_copy(
            src_ref=src, dst_ref=dst, send_sem=ssem, recv_sem=rsem,
            device_id=(e, t), device_id_type=MESH,
        )

    def lanes_to_rows(v):
        return jnp.transpose(v)

    xf = tok_ref[...].astype(F32)
    sq = xf * xf
    groups = sq[:, 0:128]
    for j in range(1, width // 128):
        groups = groups + sq[:, j * 128:(j + 1) * 128]
    mine = jnp.sum(lanes_to_rows(groups), axis=0, keepdims=True)
    part[0] = jnp.broadcast_to(mine, (8, rows))

    pl.semaphore_wait(barrier, 3 + n - 1)
    p_copies = [
        remote(part.at[0], part.at[j], p_send.at[j], p_recv.at[j], me, other)
        for j, other in ((1, partner), (2, across), (3, diag))
    ]
    for copy in p_copies:
        copy.start()

    experts = slot_row.shape[0]
    expert_of = lax.broadcasted_iota(jnp.int32, (experts, rows), 0)
    first = expert_of == ids_ref[0:1, :]
    second = expert_of == ids_ref[1:2, :]
    named = jnp.where(first | second, 1.0, 0.0)
    before = (
        lax.broadcasted_iota(jnp.int32, (rows, rows), 0)
        < lax.broadcasted_iota(jnp.int32, (rows, rows), 1)
    )
    earlier = jnp.dot(
        named.astype(BF), jnp.where(before, 1.0, 0.0).astype(BF), preferred_element_type=F32
    )
    slot_row[...] = jnp.where(named > 0.5, earlier, -1.0)
    share_row[...] = jnp.where(first, share_ref[0:1, :], 0.0) + jnp.where(
        second, share_ref[1:2, :], 0.0
    )
    slot_of = lax.broadcasted_iota(jnp.int32, (cap, rows), 0).astype(F32)

    def placed(k):
        e = peer(k)
        return slot_of == jnp.broadcast_to(slot_row[pl.ds(e, 1), :], (cap, rows))

    def place(k):
        return jnp.where(placed(k), 1.0, 0.0).astype(BF)

    for copy in p_copies:
        copy.wait_recv()
    total = part[0] + part[1] + part[2] + part[3]
    factor = lax.rsqrt(total[0:1, :] / (width * n_tp) + EPS)
    column = jnp.transpose(jnp.broadcast_to(factor, (128, rows)))
    column = jnp.concatenate([column] * (width // 128), axis=1)
    near[...] = (xf * column * gain_ref[...].astype(F32)).astype(BF)
    n_copy = remote(near, far, n_send, n_recv, me, across)
    n_copy.start()

    def a_copy(k, e):
        return remote(send_a.at[k], xs.at[k, c, x], a_send.at[k], a_recv.at[k], e, tp)

    def b_copy(k, e):
        return remote(send_b.at[k], xs.at[k, c, 1 - x], b_send.at[k], b_recv.at[k], e, tp)

    def send_near(k):
        send_a[k] = jnp.dot(place(k), near[...], preferred_element_type=F32).astype(BF)
        a_copy(k, peer(k)).start()

    def send_far(k):
        send_b[k] = jnp.dot(place(k), far[...], preferred_element_type=F32).astype(BF)
        b_copy(k, peer(k)).start()

    first_far = half + half // 2
    for k in range(half, first_far):
        send_near(k)
    for k in range(1, half):
        send_near(k)

    xs[0, c, x] = jnp.dot(place(0), near[...], preferred_element_type=F32).astype(BF)

    def weigh(k):
        e = peer(k)
        weight = jnp.where(
            placed(k), jnp.broadcast_to(share_row[pl.ds(e, 1), :], (cap, rows)), 0.0
        )
        weight = jnp.transpose(weight)
        high = weight.astype(BF)
        mix_hi[k] = high
        mix_lo[k] = (weight - high.astype(F32)).astype(BF)

    n_copy.wait_recv()
    xs[0, c, 1 - x] = jnp.dot(place(0), far[...], preferred_element_type=F32).astype(BF)

    for i in range(max(half - 1, n - first_far)):
        if i + 1 < half:
            send_far(i + 1)
        if first_far + i < n:
            send_near(first_far + i)

    def f_copy(k):
        return remote(xs.at[k, c, x], xs.at[k, c, x], f_send.at[k], f_recv.at[k], me, across)

    def f_arrival(k):
        there = xs.at[k, c, 1 - x]
        return remote(there, there, f_send.at[k], f_recv.at[k], me, across)

    def d_copy(k, core):
        ref = xs.at[k, core] if k < half else xs.at[k, core, x]
        return remote(ref, ref, d_send.at[k], d_recv.at[k], me, partner)

    def e_copy(k, core):
        ref = xs.at[k, core, 1 - x]
        return remote(ref, ref, e_send.at[k], e_recv.at[k], me, partner)

    def y_copy(k):
        return remote(ys.at[k], yd.at[k], y_send.at[k], y_recv.at[k], me, partner)

    def z_copy(k):
        return remote(zs.at[k], zx.at[k], z_send.at[k], z_recv.at[k], me, across)

    def r_copy(k):
        return remote(rs.at[k], ra.at[k], r_send.at[k], r_recv.at[k], peer(k), tp)

    def arrive(ks):
        for k in ks:
            if k:
                a_copy(k, me).wait_recv()
            if k >= half:
                f_copy(k).start()
            elif k:
                b_copy(k, me).wait_recv()
            d_copy(k, c).start()

    def pair(ks):
        for k in ks:
            y_copy(k).wait_recv()
            zs[k] = (own_y[k, 1] + yd[k, 1].astype(F32)).astype(BF)
            z_copy(k).start()
        for k in ks:
            za[k] = own_y[k, 0] + yd[k, 0].astype(F32)

    def give(ks):
        for k in ks:
            z_copy(k).wait_recv()
            result = (za[k] + zx[k].astype(F32)).astype(BF)
            if k:
                rs[k] = result
                r_copy(k).start()
            else:
                ra[0] = result

    ff = wg.shape[1]
    tile = 256 if ff % 256 == 0 else 128

    arrive(steps[0])

    @pl.loop(0, n)
    def _(k):
        weigh(k)

    for load in loads:
        load.wait()

    for step, ks in enumerate(steps):
        for k in ks:
            if k >= half:
                f_arrival(k).wait_recv()
                e_copy(k, c).start()
        if step >= 1:
            pair(steps[step - 1])
        if step >= 2:
            give(steps[step - 2])
        for k in ks:
            d_copy(k, 1 - c).wait_recv()
            if k >= half:
                e_copy(k, 1 - c).wait_recv()
        block = jnp.concatenate(
            [
                jnp.concatenate([xs[k, q % CORES, q // CORES] for q in range(n_tp)], axis=1)
                for k in ks
            ],
            axis=0,
        )
        held = cap * len(ks)
        for f in range(0, ff, tile):
            gate = jnp.dot(block, wg[:, f:f + tile], preferred_element_type=F32)
            up = jnp.dot(block, wu[:, f:f + tile], preferred_element_type=F32)
            hid[0:held, f:f + tile] = (gate / (1.0 + jnp.exp(-gate)) * up).astype(BF)
        if step + 1 < len(steps):
            arrive(steps[step + 1])
        hidden = hid[0:held, :]
        for i, q_x in enumerate((x, 1 - x)):
            y = jnp.dot(hidden, wd[q_x * CORES + 1 - c], preferred_element_type=F32).astype(BF)
            for m, k in enumerate(ks):
                ys[k, i] = y[m * cap:(m + 1) * cap]
        for k in ks:
            y_copy(k).start()
        for i, q_x in enumerate((x, 1 - x)):
            y = jnp.dot(hidden, wd[q_x * CORES + c], preferred_element_type=F32)
            for m, k in enumerate(ks):
                own_y[k, i] = y[m * cap:(m + 1) * cap]
    pair(steps[-1])
    for ks in steps[-2:]:
        give(ks)

    def mixed(k):
        back = ra[k]
        return jnp.dot(mix_hi[k], back, preferred_element_type=F32) + jnp.dot(
            mix_lo[k], back, preferred_element_type=F32
        )

    total = mixed(0)
    for k in [k for ks in steps for k in ks if k]:
        r_copy(k).wait_recv()
        total = total + mixed(k)
    out_ref[...] = total.astype(BF)

    for copy in p_copies:
        copy.wait_send()
    n_copy.wait_send()
    for k in range(n):
        d_copy(k, c).wait_send()
        y_copy(k).wait_send()
        z_copy(k).wait_send()
        if k:
            a_copy(k, me).wait_send()
            r_copy(k).wait_send()
        if 0 < k < half:
            b_copy(k, me).wait_send()
        if k >= half:
            f_copy(k).wait_send()
            e_copy(k, c).wait_send()


def order(n):
    half, quarter = n // 2, n // 4
    starts = (0, half, quarter, half + quarter)
    return [tuple(range(i, i + 2)) for s in starts for i in range(s, s + quarter, 2)]


def routed(n, n_tp, tokens, norm_gain, expert_ids, gate_share, gate_weight, up_weight, down_weight):
    rows, width = tokens.shape
    experts = n * gate_weight.shape[0]
    cap = 4 * rows // experts
    depth, ff = gate_weight.shape[1:]
    vmem = pl.BlockSpec(memory_space=pltpu.VMEM)
    hbm = pl.BlockSpec(memory_space=pltpu.HBM)
    dma = pltpu.SemaphoreType.DMA
    return pl.pallas_call(
        functools.partial(fused, n, n_tp, order(n)),
        out_shape=jax.ShapeDtypeStruct((rows, width), BF),
        in_specs=[vmem] * 4 + [hbm] * 3,
        out_specs=vmem,
        scratch_shapes=[
            pltpu.VMEM((depth, ff), BF),
            pltpu.VMEM((depth, ff), BF),
            pltpu.VMEM((n_tp, ff, width), BF),
            pltpu.VMEM((4, 8, rows), F32),
            pltpu.VMEM((rows, width), BF),
            pltpu.VMEM((rows, width), BF),
            pltpu.VMEM((experts, rows), F32),
            pltpu.VMEM((experts, rows), F32),
            pltpu.VMEM((n, cap, width), BF),
            pltpu.VMEM((n, cap, width), BF),
            pltpu.VMEM((n, CORES, n_tp // CORES, cap, width), BF),
            pltpu.VMEM((2 * cap, ff), BF),
            pltpu.VMEM((n, 2, cap, width), F32),
            pltpu.VMEM((n, 2, cap, width), BF),
            pltpu.VMEM((n, 2, cap, width), BF),
            pltpu.VMEM((n, cap, width), F32),
            pltpu.VMEM((n, cap, width), BF),
            pltpu.VMEM((n, cap, width), BF),
            pltpu.VMEM((n, cap, width), BF),
            pltpu.VMEM((n, cap, width), BF),
            pltpu.VMEM((n, rows, cap), BF),
            pltpu.VMEM((n, rows, cap), BF),
            dma((2 + n_tp,)),
            dma((4,)), dma((4,)),
            dma, dma,
            dma((n,)), dma((n,)),
            dma((n,)), dma((n,)),
            dma((n,)), dma((n,)),
            dma((n,)), dma((n,)),
            dma((n,)), dma((n,)),
            dma((n,)), dma((n,)),
            dma((n,)), dma((n,)),
            dma((n,)), dma((n,)),
        ],
        compiler_params=pltpu.CompilerParams(
            collective_id=0, has_side_effects=True, vmem_limit_bytes=56 * 1024 * 1024
        ),
    )(
        tokens, norm_gain.reshape(1, width), expert_ids.T, gate_share.T,
        gate_weight, up_weight, down_weight,
    )


def shards(n, n_tp, *args):
    tokens, gate_weight = args[0], args[4]
    rows, width = tokens.shape
    cap = 4 * rows // (n * gate_weight.shape[0])
    fits = (
        n_tp == 2 * CORES and n >= 8 and n & (n - 1) == 0 and gate_weight.shape[0] == 1 and rows % 128 == 0
        and width % 128 == 0 and gate_weight.shape[2] % 128 == 0 and cap % 128 == 0
    )
    return routed(n, n_tp, *args) if fits else plain(*args)


def solution(mesh):
    body = functools.partial(shards, mesh.shape["ep"], mesh.shape["tp"])
    in_specs = (
        P("ep", "tp"),
        P("tp"),
        P("ep", None),
        P("ep", None),
        P("ep", None, "tp"),
        P("ep", None, "tp"),
        P("ep", "tp", None),
    )
    out_specs = P("ep", "tp")
    return jax.shard_map(body, mesh=mesh, in_specs=in_specs, out_specs=out_specs, check_vma=False)
```

profile of v0, /device:TPU:8, one launch (start us, length us, event | category | flops | bytes accessed | tf_op | source)
XLA Modules:
  0.0 82.6 jit_solution(1565360088954914010)
XLA Ops:
  0.0 1.3 %reshape.3.gain_ref = bf16[1,512]{1,0:T(2,128)(2,1)} reshape(bf16[512]{0:T(512)(128)(2,1)} %param.8) | data formatting | bytes 2048 | tf_op jit(solution)/shard_map/reshape | solution.py:397
  1.3 79.6 %shard_map.73 = bf16[256,512]{1,0:T(8,128)(2,1)} custom-call(bf16[256,512]{1,0:T(8,128)(2,1)} %tok_ref.1, bf16[1,512]{1,0:T(2,128)(2,1)} %reshape.3.gain_ref, s32[2,256]{1,0:T(2,128)} %bitcast.2, f32[2,256]{1,0:T(2,128)} %bitcast.3, bf16[1,2048,1024]{2,1,0:T(8,128)(2,1)} %wg_hbm.1, bf16[1,2048,1024]{2,1,0:T(8,128)(2,1)} %wu_hbm.1, bf16[1,1024,2048]{2,1,0:T(8,128)(2,1)} %wd_hbm.1), custom_call_target="tpu_custom_call" | custom-call | tf_op jit(solution)/shard_map/pallas_call | solution.py:353
  80.9 1.7 %copy.9 = bf16[256,512]{1,0:T(8,128)(2,1)} copy(bf16[256,512]{1,0:T(8,128)(2,1)} %shard_map.73) | data formatting | bytes 524288
where the time goes:
time: 83.1 us; the launch traced here: 82.6 us
  Pallas kernels  79.6 us (96%)
  local copies, waits for them, and re-layouts  2.93 us (4%)
    pallas_call x1, Pallas kernels, routed(): pl.pallas_call(functools.partial(fused, n, n_tp, order(n)), out_shape=jax...  79.6 us
    unnamed x1, local copies, waits for them, and re-layouts  1.67 us

commit v1 on v0

v1 whole, which is shorter than its diff:
```python
import functools
import jax
import jax.numpy as jnp
from jax import lax
from jax.experimental import pallas as pl
from jax.experimental.pallas import tpu as pltpu
from jax.sharding import PartitionSpec as P

D = 2048


EPS = 1e-06
MESH = pl.DeviceIdType.MESH
BF = jnp.bfloat16
F32 = jnp.float32
CORES = 2
LINE = 2
mark = jax.named_scope
SENDS = (
    "6/2", "4/3", "2/1", "3/4", "1/6", "7/5", "5/7",
)
NEAR = 3
LAST = "5"
ORDER = (
    "take:0", "take:1", "pass:0", "<take:6",
    "load:0", "ready:0", "norm:0", "gu0:0", "gu1:0", "gu2:0", "gu3:0", "away:0", "here:0",
    ">take:6", "<take:2", "pass:1",
    "ready:1", "norm:1", "gu0:1", "gu1:1", "home:0", "<take:3", ">take:4", "gu2:1", "gu3:1",
    "<pass:6", ">take:2", "away:1", "here:1", ">pass:6",
    "ready:6", "norm:6", "gu0:6", "home:1", "gu1:6", ">take:3", "gu2:6", "gu3:6", "pass:2/4",
    "away:6", "<take:4", "here:6",
    "ready:2/4", "norm:2/4", "gu0:2/4", "pair:6", "gu1:2/4", "gu2:2/4", "gu3:2/4", "pass:3/2",
    "away:2/4", "take:7", "here:2/4",
    "ready:3/2", "norm:3/2", "gu0:3/2", "<home:2", ">pair:4", "gu1:3/2", ">take:5", "gu2:3/2",
    "gu3:3/2", ">pass:3", "<pass:4", "away:3/2", "here:3/2", "<take:5",
    "ready:4/3", "norm:4/3", "gu0:4/3", ">home:2", ">give:6", "gu1:4/3", "<give:6", "gu2:4/3",
    "gu3:4/3", "pass:7", "away:4/3", "here:4/3", "<pair:3",
    "ready:7", "norm:7", "gu0:7", "<pair:4", ">pair:3", "gu1:7", ">give:4", "gu2:7", "gu3:7",
    ">pass:5", "away:7", "here:7", "<pass:5",
    "ready:5", "norm:5", "gu0:5", "pair:7", "gu1:5", "gu2:5", "gu3:5", "away:5", "<give:4",
    "<give:3", "here:5",
    "collect:1", "collect:2", "pair:5", ">give:3", "give:7", "swap:0", "give:5", "gather:0",
    "mix:6", "mix:4", "mix:3", "mix:7",
)


def plain(tokens, norm_gain, expert_ids, gate_share, gate_weight, up_weight, down_weight):
    n_expdev = lax.axis_size("ep")
    exp_local = gate_weight.shape[0]
    experts = exp_local * n_expdev
    tok_rows = tokens.shape[0]
    slot_cap = 4 * tok_rows // experts
    flat_ids = expert_ids.reshape(-1)
    onehot = (flat_ids[:, None] == jnp.arange(experts, dtype=jnp.int32)[None, :]).astype(jnp.int32)
    slots = jnp.sum((jnp.cumsum(onehot, axis=0) - onehot) * onehot, axis=1)
    target = flat_ids * slot_cap + slots
    values = tokens.astype(jnp.float32)
    squares = lax.psum(jnp.sum(values * values, axis=1), "tp")
    factor = lax.rsqrt(squares / D + EPS)
    normed = (values * factor[:, None] * norm_gain.astype(jnp.float32)[None, :]).astype(
        jnp.bfloat16
    )
    rows = jnp.repeat(normed, 2, axis=0)
    buffer = jnp.zeros((experts * slot_cap, normed.shape[1]), jnp.bfloat16).at[target].set(rows)
    buffer = buffer.reshape(n_expdev, exp_local, slot_cap, normed.shape[1])
    arrived = lax.all_to_all(buffer, "ep", split_axis=0, concat_axis=0, tiled=True)
    piece = lax.all_gather(arrived, "tp", axis=3, tiled=True)
    first = jnp.einsum("secd,edf->secf", piece, gate_weight, preferred_element_type=jnp.float32)
    second = jnp.einsum("secd,edf->secf", piece, up_weight, preferred_element_type=jnp.float32)
    hidden = (jax.nn.silu(first) * second).astype(jnp.bfloat16)
    width_local = D // lax.axis_size("tp")
    term = jnp.einsum("secf,efd->dsec", hidden, down_weight, preferred_element_type=jnp.float32)
    summed = lax.psum_scatter(
        term.reshape(lax.axis_size("tp") * width_local, n_expdev * exp_local * slot_cap).astype(
            jnp.bfloat16
        ),
        "tp",
        scatter_dimension=0,
        tiled=True,
    )
    results = summed.reshape(width_local, n_expdev, exp_local, slot_cap)
    results = jnp.transpose(results, (1, 2, 3, 0))
    returned = lax.all_to_all(results, "ep", split_axis=0, concat_axis=0, tiled=True)
    flat_back = returned.reshape(experts * slot_cap, width_local)
    picked = flat_back[target].astype(jnp.float32).reshape(tok_rows, 2, width_local)
    return jnp.sum(picked * gate_share[:, :, None], axis=1).astype(jnp.bfloat16)


def fused(
    n, n_tp,
    tok_hbm, gain_hbm, ids_hbm, share_hbm, wg_hbm, wu_hbm, wd_hbm,
    out_ref,
    tok, gain, ids, share, wg, wu, wd, gains, slot_row, share_row, send_a, xs, block,
    hid, own_y, ys, yd, za, zs, zx, rs, ra, ns, na, away_part, far_part, sums, mix_hi, mix_lo,
    in_sem, w_sem, g_send, g_recv, a_send, a_recv,
    f_send, f_recv, d_send, d_recv, e_send, e_recv, y_send, y_recv, z_send, z_recv, r_send, r_recv,
    h_send, h_recv,
):
    me = lax.axis_index("ep")
    tp = lax.axis_index("tp")
    x, c = tp // CORES, tp % CORES
    partner = x * CORES + (1 - c)
    across = (1 - x) * CORES + c
    diag = (1 - x) * CORES + (1 - c)
    rows, width = tok.shape
    cap = send_a.shape[1]
    half = n // 2

    z, y = me // LINE, me % LINE
    depth = n // LINE
    high = z // (depth // 2)
    outer = (z + high + 1) % 2
    beside = z + 1 - 2 * (z % 2)
    inner_there = depth // 2 - high
    outer_there = (1 - high) * (depth - 1)

    def either(pair, value=lambda k: k):
        a, b = value(pair[0]), value(pair[1])
        return a if pair[0] == pair[1] else outer * a + (1 - outer) * b

    def peer_of(k):
        level = (z, beside, inner_there, outer_there)[k // LINE]
        return level * LINE + (1 - y if k % LINE else y)

    def there_of(k):
        return k if k < half else half + LINE * outer + k % LINE

    def at(k):
        return either(k)

    def peer(k):
        return either(k, peer_of)

    def there(k):
        return either(k, there_of)

    barrier = pltpu.get_barrier_semaphore()
    for k in range(1, n):
        pl.semaphore_signal(barrier, inc=1, device_id=(peer_of(k), tp), device_id_type=MESH)
    for other in (partner, across, diag):
        pl.semaphore_signal(barrier, inc=1, device_id=(me, other), device_id_type=MESH)

    inputs = [
        pltpu.make_async_copy(src, dst, in_sem.at[i])
        for i, (src, dst) in enumerate(
            ((tok_hbm, tok), (ids_hbm, ids), (share_hbm, share), (gain_hbm, gain))
        )
    ]
    for load in inputs:
        load.start()
    def remote(src, dst, ssem, rsem, e, t):
        return pltpu.make_async_remote_copy(
            src_ref=src, dst_ref=dst, send_sem=ssem, recv_sem=rsem,
            device_id=(e, t), device_id_type=MESH,
        )

    for load in inputs:
        load.wait()
    loads = [
        pltpu.make_async_copy(wg_hbm.at[0], wg, w_sem.at[0]),
        pltpu.make_async_copy(wu_hbm.at[0], wu, w_sem.at[1]),
    ] + [
        pltpu.make_async_copy(wd_hbm.at[0, :, pl.ds(q * width, width)], wd.at[q], w_sem.at[2 + q])
        for q in range(n_tp)
    ]

    experts = slot_row.shape[0]
    expert_of = lax.broadcasted_iota(jnp.int32, (experts, rows), 0)
    first = expert_of == ids[0:1, :]
    second = expert_of == ids[1:2, :]
    named = jnp.where(first | second, 1.0, 0.0)
    before = (
        lax.broadcasted_iota(jnp.int32, (rows, rows), 0)
        < lax.broadcasted_iota(jnp.int32, (rows, rows), 1)
    )
    earlier = jnp.dot(
        named.astype(BF), jnp.where(before, 1.0, 0.0).astype(BF), preferred_element_type=F32
    )
    slot_row[...] = jnp.where(named > 0.5, earlier, -1.0)
    share_row[...] = jnp.where(first, share[0:1, :], 0.0) + jnp.where(
        second, share[1:2, :], 0.0
    )
    slot_of = lax.broadcasted_iota(jnp.int32, (cap, rows), 0).astype(F32)

    def placed(k):
        return slot_of == jnp.broadcast_to(slot_row[pl.ds(peer(k), 1), :], (cap, rows))

    def place(k):
        return jnp.dot(
            jnp.where(placed(k), 1.0, 0.0).astype(BF), tok[...], preferred_element_type=F32
        ).astype(BF)

    def a_copy(k):
        s = there(k)
        return remote(
            send_a.at[at(k)], xs.at[s, c, x], a_send.at[at(k)], a_recv.at[s], peer(k), tp
        )

    def a_arrival(k):
        s = at(k)
        return remote(send_a.at[s], xs.at[s, c, x], a_send.at[s], a_recv.at[s], peer(k), tp)

    def send(k):
        send_a[at(k)] = place(k)
        a_copy(k).start()

    def f_copy(k):
        ref = xs.at[at(k), c, x]
        return remote(ref, ref, f_send.at[at(k)], f_recv.at[at(k)], me, across)

    def weigh(k):
        weight = jnp.where(
            placed(k), jnp.broadcast_to(share_row[pl.ds(peer(k), 1), :], (cap, rows)), 0.0
        )
        weight = jnp.transpose(weight)
        high_part = weight.astype(BF)
        mix_hi[at(k)] = high_part
        mix_lo[at(k)] = (weight - high_part.astype(F32)).astype(BF)

    sends = [slot_pair(word) for word in SENDS]
    ahead = sends[:2]
    for k in ahead:
        send_a[at(k)] = place(k)
    own = (0, 0)
    xs[0, c, x] = place(own)
    gains[pl.ds(tp, 1)] = jnp.broadcast_to(
        gain[...].astype(F32).reshape(1, 1, width), (1, 1, width)
    )

    with mark("barrier"):
        pl.semaphore_wait(barrier, n_tp - 1 + n - 1)
    g_copies = [
        remote(gains.at[tp], gains.at[tp], g_send.at[j], g_recv.at[j], me, other)
        for j, other in enumerate((partner, across, diag))
    ]
    g_arrivals = [
        remote(gains.at[other], gains.at[other], g_send.at[j], g_recv.at[j], me, other)
        for j, other in enumerate((partner, across, diag))
    ]
    for copy in g_copies:
        copy.start()
    for k in ahead:
        a_copy(k).start()
    f_copy(own).start()
    for k in sends[2:]:
        send(k)

    for load in loads:
        load.start()

    with mark("weigh"):
        for k in range(n):
            weigh((k, k))

    def f_arrival(k):
        ref = xs.at[at(k), c, 1 - x]
        return remote(ref, ref, f_send.at[at(k)], f_recv.at[at(k)], me, across)

    def d_copy(k, core):
        ref = xs.at[at(k), core, x]
        return remote(ref, ref, d_send.at[at(k)], d_recv.at[at(k)], me, partner)

    def e_copy(k, core):
        ref = xs.at[at(k), core, 1 - x]
        return remote(ref, ref, e_send.at[at(k)], e_recv.at[at(k)], me, partner)

    def y_copy(k):
        s = at(k)
        return remote(ys.at[s], yd.at[s], y_send.at[s], y_recv.at[s], me, partner)

    def z_copy(k):
        s = at(k)
        return remote(zs.at[s], zx.at[s], z_send.at[s], z_recv.at[s], me, across)

    def h_copy(k):
        s = at(k)
        return remote(ns.at[s], na.at[s], r_send.at[s], r_recv.at[s], peer(k), tp)

    x_copy = remote(away_part, far_part, h_send, h_recv, me, across)

    def home(k):
        s = at(k)
        y_copy(k).wait_recv()
        for i in (1, 0):
            result = (own_y[s, i] + yd[s, i].astype(F32)).astype(BF)
            if k == own:
                na[0, i] = result
            else:
                ns[s, i] = result
        if k != own:
            h_copy(k).start()

    def r_copy(k):
        s = there(k)
        return remote(rs.at[at(k)], ra.at[s], r_send.at[at(k)], r_recv.at[s], peer(k), tp)

    def r_arrival(k):
        s = at(k)
        return remote(rs.at[s], ra.at[s], r_send.at[s], r_recv.at[s], peer(k), tp)

    def take(k):
        if k != own:
            a_arrival(k).wait_recv()
            f_copy(k).start()
        d_copy(k, c).start()

    def pass_on(k):
        f_arrival(k).wait_recv()
        e_copy(k, c).start()

    def ready(k):
        d_copy(k, 1 - c).wait_recv()
        e_copy(k, 1 - c).wait_recv()

    def pair(k):
        s = at(k)
        y_copy(k).wait_recv()
        zs[s] = (own_y[s, 1] + yd[s, 1].astype(F32)).astype(BF)
        z_copy(k).start()
        za[s] = own_y[s, 0] + yd[s, 0].astype(F32)

    def give(k):
        s = at(k)
        z_copy(k).wait_recv()
        rs[s] = (za[s] + zx[s].astype(F32)).astype(BF)
        r_copy(k).start()

    ff = wg.shape[1]
    tile = 256 if ff % 256 == 0 else 128

    def normalize(k):
        s = at(k)
        pieces = [xs[s, q % CORES, q // CORES].astype(F32) for q in range(n_tp)]
        lanes = None
        for piece in pieces:
            square = piece * piece
            for j in range(0, width, 128):
                part = square[:, j:j + 128]
                lanes = part if lanes is None else lanes + part
        total = jnp.sum(lanes, axis=1, keepdims=True)
        factor = lax.rsqrt(total / (width * n_tp) + EPS)
        for q, piece in enumerate(pieces):
            block[:, q * width:(q + 1) * width] = (
                piece * factor * gains[q]
            ).astype(BF)

    def up_gate(k, part):
        for f in range(part * ff // 4, (part + 1) * ff // 4, tile):
            gate = jnp.dot(block[...], wg[:, f:f + tile], preferred_element_type=F32)
            up = jnp.dot(block[...], wu[:, f:f + tile], preferred_element_type=F32)
            hid[:, f:f + tile] = (gate / (1.0 + jnp.exp(-gate)) * up).astype(BF)

    def down_away(k):
        s = at(k)
        for i, q_x in ((1, 1 - x), (0, x)):
            ys[s, i] = jnp.dot(
                hid[...], wd[q_x * CORES + 1 - c], preferred_element_type=F32
            ).astype(BF)
        y_copy(k).start()

    def down_here(k):
        s = at(k)
        for i, q_x in ((1, 1 - x), (0, x)):
            own_y[s, i] = jnp.dot(hid[...], wd[q_x * CORES + c], preferred_element_type=F32)

    def mixed(k, back):
        return jnp.dot(mix_hi[at(k)], back, preferred_element_type=F32) + jnp.dot(
            mix_lo[at(k)], back, preferred_element_type=F32
        )

    def collect(k):
        h_copy(k).wait_recv()

    def swap(k):
        total = None
        for s in range(NEAR):
            part = mixed((s, s), na[s, 1])
            total = part if total is None else total + part
        away_part[...] = total.astype(BF)
        x_copy.start()

    def gather(k):
        total = None
        for s in range(NEAR):
            part = mixed((s, s), na[s, 0])
            total = part if total is None else total + part
        sums[...] = total

    def far_mix(k):
        r_arrival(k).wait_recv()
        sums[...] = sums[...] + mixed(k, ra[at(k)])

    with mark("gains"):
        for copy in g_arrivals:
            copy.wait_recv()

    def weights(k):
        for load in loads:
            load.wait()

    def only(role, action):
        def run(k):
            @pl.when(outer == role)
            def _():
                action(k)
        return run

    todo = {
        "take": take, "pass": pass_on, "ready": ready, "norm": normalize, "load": weights,
        "away": down_away, "here": down_here, "pair": pair, "give": give,
        "home": home, "collect": collect, "swap": swap, "gather": gather, "mix": far_mix,
    }
    for part in range(4):
        todo["gu%d" % part] = functools.partial(up_gate, part=part)
    for word in ORDER:
        name, ks = word.split(":")
        k = slot_pair(ks)
        action = todo[name.strip("<>")]
        if name[0] == "<":
            action = only(1, action)
        elif name[0] == ">":
            action = only(0, action)
        with mark("%s_%s" % (name, ks.replace("/", "i"))):
            action(k)

    last = slot_pair(LAST)
    with mark("last"):
        r_arrival(last).wait_recv()
    total = sums[...] + mixed(last, ra[at(last)])
    with mark("swapped"):
        x_copy.wait_recv()
    out_ref[...] = (total + far_part[...].astype(F32)).astype(BF)

    with mark("sends"):
        for copy in g_copies:
            copy.wait_send()
        for k in [(k, k) for k in range(n)]:
            f_copy(k).wait_send()
            d_copy(k, c).wait_send()
            e_copy(k, c).wait_send()
            y_copy(k).wait_send()
            if k != own:
                a_copy(k).wait_send()
            if k[0] >= NEAR:
                z_copy(k).wait_send()
                r_copy(k).wait_send()
            elif k != own:
                h_copy(k).wait_send()
        x_copy.wait_send()


def slot_pair(word):
    parts = word.split("/")
    return int(parts[0]), int(parts[-1])


def routed(n, n_tp, tokens, norm_gain, expert_ids, gate_share, gate_weight, up_weight, down_weight):
    rows, width = tokens.shape
    experts = n * gate_weight.shape[0]
    cap = 4 * rows // experts
    depth, ff = gate_weight.shape[1:]
    hbm = pl.BlockSpec(memory_space=pltpu.HBM)
    dma = pltpu.SemaphoreType.DMA
    return pl.pallas_call(
        functools.partial(fused, n, n_tp),
        out_shape=pltpu.VMEM((rows, width), BF),
        in_specs=[hbm] * 7,
        out_specs=pl.BlockSpec(memory_space=pltpu.VMEM),
        scratch_shapes=[
            pltpu.VMEM((rows, width), BF),
            pltpu.VMEM((width,), BF),
            pltpu.VMEM((2, rows), jnp.int32),
            pltpu.VMEM((2, rows), F32),
            pltpu.VMEM((depth, ff), BF),
            pltpu.VMEM((depth, ff), BF),
            pltpu.VMEM((n_tp, ff, width), BF),
            pltpu.VMEM((n_tp, 1, width), F32),
            pltpu.VMEM((experts, rows), F32),
            pltpu.VMEM((experts, rows), F32),
            pltpu.VMEM((n, cap, width), BF),
            pltpu.VMEM((n, CORES, n_tp // CORES, cap, width), BF),
            pltpu.VMEM((cap, depth), BF),
            pltpu.VMEM((cap, ff), BF),
            pltpu.VMEM((n, 2, cap, width), F32),
            pltpu.VMEM((n, 2, cap, width), BF),
            pltpu.VMEM((n, 2, cap, width), BF),
            pltpu.VMEM((n, cap, width), F32),
            pltpu.VMEM((n, cap, width), BF),
            pltpu.VMEM((n, cap, width), BF),
            pltpu.VMEM((n, cap, width), BF),
            pltpu.VMEM((n, cap, width), BF),
            pltpu.VMEM((n // 2, 2, cap, width), BF),
            pltpu.VMEM((n // 2, 2, cap, width), BF),
            pltpu.VMEM((rows, width), BF),
            pltpu.VMEM((rows, width), BF),
            pltpu.VMEM((rows, width), F32),
            pltpu.VMEM((n, rows, cap), BF),
            pltpu.VMEM((n, rows, cap), BF),
            dma((4,)), dma((2 + n_tp,)),
            dma((3,)), dma((3,)),
            dma((n,)), dma((n,)),
            dma((n,)), dma((n,)),
            dma((n,)), dma((n,)),
            dma((n,)), dma((n,)),
            dma((n,)), dma((n,)),
            dma((n,)), dma((n,)),
            dma((n,)), dma((n,)),
            dma, dma,
        ],
        compiler_params=pltpu.CompilerParams(
            collective_id=0, has_side_effects=True, vmem_limit_bytes=56 * 1024 * 1024
        ),
    )(
        tokens, norm_gain, expert_ids.T, gate_share.T,
        gate_weight, up_weight, down_weight,
    )


def shards(n, n_tp, *args):
    tokens, gate_weight = args[0], args[4]
    rows, width = tokens.shape
    cap = 4 * rows // (n * gate_weight.shape[0])
    fits = (
        n_tp == 2 * CORES and n == 4 * LINE and gate_weight.shape[0] == 1 and rows % 128 == 0
        and width % 128 == 0 and gate_weight.shape[2] % 128 == 0 and cap % 128 == 0
    )
    return routed(n, n_tp, *args) if fits else plain(*args)


def solution(mesh):
    body = functools.partial(shards, mesh.shape["ep"], mesh.shape["tp"])
    in_specs = (
        P("ep", "tp"),
        P("tp"),
        P("ep", None),
        P("ep", None),
        P("ep", None, "tp"),
        P("ep", None, "tp"),
        P("ep", "tp", None),
    )
    out_specs = P("ep", "tp")
    return jax.shard_map(body, mesh=mesh, in_specs=in_specs, out_specs=out_specs, check_vma=False)
```

time: 83.1 us -> 58.7 us (0.71)
  Pallas kernels: 79.6 us -> 57.9 us
  local copies, waits for them, and re-layouts: 2.93 us -> 0.71 us
    pallas_call x1, Pallas kernels: 79.6 us -> 57.9 us  [routed(): pl.pallas_call(functools.partial(fused, n, n_tp), out_shape=pltpu.VMEM((r...]
    reshape x1 -> x0, local copies, waits for them, and re-layouts: 1.26 us -> none  [routed(): norm_gain.reshape(1, width)]
    unnamed x1, local copies, waits for them, and re-layouts: 1.67 us -> 0.71 us
where the time goes in v1:
time: 58.7 us; the launch traced here: 58.6 us
  Pallas kernels  57.9 us (99%)
  local copies, waits for them, and re-layouts  0.71 us (1%)
    pallas_call x1, Pallas kernels, routed(): pl.pallas_call(functools.partial(fused, n, n_tp), out_shape=pltpu.VMEM((r...  57.9 us

profile of v1, /device:TPU:8, one launch (start us, length us, event | category | flops | bytes accessed | tf_op | source)
XLA Modules:
  0.0 58.6 jit_solution(12549963127615644128)
XLA Ops:
  0.0 57.9 %shard_map.73 = bf16[256,512]{1,0:T(8,128)(2,1)S(1)} custom-call(bf16[256,512]{1,0:T(8,128)(2,1)} %tok_hbm.1, bf16[512]{0:T(512)(128)(2,1)} %gain_hbm.1, s32[2,256]{1,0:T(2,128)} %bitcast.2, f32[2,256]{1,0:T(2,128)} %bitcast.3, bf16[1,2048,1024]{2,1,0:T(8,128)(2,1)} %wg_hbm.1, bf16[1,2048,1024]{2,1,0:T(8,128)(2,1)} %wu_hbm.1, bf16[1,1024,2048]{2,1,0:T(8,128)(2,1)} %wd_hbm.1), custom_call_target="tpu_custom_call" | custom-call | tf_op jit(solution)/shard_map/pallas_call | solution.py:464
  57.9 0.7 %copy.9 = bf16[256,512]{1,0:T(8,128)(2,1)} copy(bf16[256,512]{1,0:T(8,128)(2,1)S(1)} %shard_map.73) | data formatting | bytes 524288

commit v2 on v1

--- a/solution.py
+++ b/solution.py
@@ -27,19 +27,19 @@
     ">take:6", "<take:2", "pass:1",
     "ready:1", "norm:1", "gu0:1", "gu1:1", "home:0", "<take:3", ">take:4", "gu2:1", "gu3:1",
     "<pass:6", ">take:2", "away:1", "here:1", ">pass:6",
-    "ready:6", "norm:6", "gu0:6", "home:1", "gu1:6", ">take:3", "gu2:6", "gu3:6", "pass:2/4",
-    "away:6", "<take:4", "here:6",
+    "ready:6", "norm:6", "gu0:6", "home:1", "gu1:6", ">take:3", "gu2:6", "<take:4", "gu3:6",
+    "pass:2/4", "away:6", "here:6",
     "ready:2/4", "norm:2/4", "gu0:2/4", "pair:6", "gu1:2/4", "gu2:2/4", "gu3:2/4", "pass:3/2",
-    "away:2/4", "take:7", "here:2/4",
-    "ready:3/2", "norm:3/2", "gu0:3/2", "<home:2", ">pair:4", "gu1:3/2", ">take:5", "gu2:3/2",
-    "gu3:3/2", ">pass:3", "<pass:4", "away:3/2", "here:3/2", "<take:5",
-    "ready:4/3", "norm:4/3", "gu0:4/3", ">home:2", ">give:6", "gu1:4/3", "<give:6", "gu2:4/3",
-    "gu3:4/3", "pass:7", "away:4/3", "here:4/3", "<pair:3",
-    "ready:7", "norm:7", "gu0:7", "<pair:4", ">pair:3", "gu1:7", ">give:4", "gu2:7", "gu3:7",
-    ">pass:5", "away:7", "here:7", "<pass:5",
-    "ready:5", "norm:5", "gu0:5", "pair:7", "gu1:5", "gu2:5", "gu3:5", "away:5", "<give:4",
-    "<give:3", "here:5",
-    "collect:1", "collect:2", "pair:5", ">give:3", "give:7", "swap:0", "give:5", "gather:0",
+    "away:2/4", "take:7", "here:2/4", "<pass:4",
+    "ready:4/2", "norm:4/2", "gu0:4/2", "<home:2", ">take:5", ">pair:4", "gu1:4/2", "gu2:4/2",
+    "gu3:4/2", ">pass:3", "away:4/2", "here:4/2", "<give:6", "<take:5",
+    "ready:3", "norm:3", "gu0:3", "<pair:4", ">home:2", ">give:6", "gu1:3", "gu2:3", "gu3:3",
+    ">pass:7", "away:3", "here:3", "<pass:7",
+    "ready:7", "norm:7", "gu0:7", "pair:3", "gu1:7", "gu2:7", "gu3:7", "pass:5", "<give:4",
+    "away:7", "here:7",
+    "ready:5", "norm:5", "gu0:5", "pair:7", ">give:4", "gu1:5", "gu2:5", "gu3:5", "away:5",
+    ">give:3", "here:5",
+    "pair:5", "<give:3", "give:7", "collect:1", "collect:2", "swap:0", "give:5", "gather:0",
     "mix:6", "mix:4", "mix:3", "mix:7",
 )
 
@@ -94,7 +94,7 @@
     hid, own_y, ys, yd, za, zs, zx, rs, ra, ns, na, away_part, far_part, sums, mix_hi, mix_lo,
     in_sem, w_sem, g_send, g_recv, a_send, a_recv,
     f_send, f_recv, d_send, d_recv, e_send, e_recv, y_send, y_recv, z_send, z_recv, r_send, r_recv,
-    h_send, h_recv,
+    h_send, h_recv, n_send,
 ):
     me = lax.axis_index("ep")
     tp = lax.axis_index("tp")
@@ -193,12 +193,12 @@
     def a_copy(k):
         s = there(k)
         return remote(
-            send_a.at[at(k)], xs.at[s, c, x], a_send.at[at(k)], a_recv.at[s], peer(k), tp
+            send_a.at[at(k)], xs.at[s, c, x], a_send, a_recv.at[s], peer(k), tp
         )
 
     def a_arrival(k):
         s = at(k)
-        return remote(send_a.at[s], xs.at[s, c, x], a_send.at[s], a_recv.at[s], peer(k), tp)
+        return remote(send_a.at[s], xs.at[s, c, x], a_send, a_recv.at[s], peer(k), tp)
 
     def send(k):
         send_a[at(k)] = place(k)
@@ -206,7 +206,7 @@
 
     def f_copy(k):
         ref = xs.at[at(k), c, x]
-        return remote(ref, ref, f_send.at[at(k)], f_recv.at[at(k)], me, across)
+        return remote(ref, ref, f_send, f_recv.at[at(k)], me, across)
 
     def weigh(k):
         weight = jnp.where(
@@ -230,11 +230,11 @@
     with mark("barrier"):
         pl.semaphore_wait(barrier, n_tp - 1 + n - 1)
     g_copies = [
-        remote(gains.at[tp], gains.at[tp], g_send.at[j], g_recv.at[j], me, other)
+        remote(gains.at[tp], gains.at[tp], g_send, g_recv.at[j], me, other)
         for j, other in enumerate((partner, across, diag))
     ]
     g_arrivals = [
-        remote(gains.at[other], gains.at[other], g_send.at[j], g_recv.at[j], me, other)
+        remote(gains.at[other], gains.at[other], g_send, g_recv.at[j], me, other)
         for j, other in enumerate((partner, across, diag))
     ]
     for copy in g_copies:
@@ -254,27 +254,27 @@
 
     def f_arrival(k):
         ref = xs.at[at(k), c, 1 - x]
-        return remote(ref, ref, f_send.at[at(k)], f_recv.at[at(k)], me, across)
+        return remote(ref, ref, f_send, f_recv.at[at(k)], me, across)
 
     def d_copy(k, core):
         ref = xs.at[at(k), core, x]
-        return remote(ref, ref, d_send.at[at(k)], d_recv.at[at(k)], me, partner)
+        return remote(ref, ref, d_send, d_recv.at[at(k)], me, partner)
 
     def e_copy(k, core):
         ref = xs.at[at(k), core, 1 - x]
-        return remote(ref, ref, e_send.at[at(k)], e_recv.at[at(k)], me, partner)
+        return remote(ref, ref, e_send, e_recv.at[at(k)], me, partner)
 
     def y_copy(k):
         s = at(k)
-        return remote(ys.at[s], yd.at[s], y_send.at[s], y_recv.at[s], me, partner)
+        return remote(ys.at[s], yd.at[s], y_send, y_recv.at[s], me, partner)
 
     def z_copy(k):
         s = at(k)
-        return remote(zs.at[s], zx.at[s], z_send.at[s], z_recv.at[s], me, across)
+        return remote(zs.at[s], zx.at[s], z_send, z_recv.at[s], me, across)
 
     def h_copy(k):
         s = at(k)
-        return remote(ns.at[s], na.at[s], r_send.at[s], r_recv.at[s], peer(k), tp)
+        return remote(ns.at[s], na.at[s], n_send, r_recv.at[s], peer(k), tp)
 
     x_copy = remote(away_part, far_part, h_send, h_recv, me, across)
 
@@ -292,11 +292,11 @@
 
     def r_copy(k):
         s = there(k)
-        return remote(rs.at[at(k)], ra.at[s], r_send.at[at(k)], r_recv.at[s], peer(k), tp)
+        return remote(rs.at[at(k)], ra.at[s], r_send, r_recv.at[s], peer(k), tp)
 
     def r_arrival(k):
         s = at(k)
-        return remote(rs.at[s], ra.at[s], r_send.at[s], r_recv.at[s], peer(k), tp)
+        return remote(rs.at[s], ra.at[s], r_send, r_recv.at[s], peer(k), tp)
 
     def take(k):
         if k != own:
@@ -424,29 +424,22 @@
             action(k)
 
     last = slot_pair(LAST)
+    with mark("swapped"):
+        x_copy.wait_recv()
+    sums[...] = sums[...] + far_part[...].astype(F32)
     with mark("last"):
         r_arrival(last).wait_recv()
-    total = sums[...] + mixed(last, ra[at(last)])
-    with mark("swapped"):
-        x_copy.wait_recv()
-    out_ref[...] = (total + far_part[...].astype(F32)).astype(BF)
+    out_ref[...] = (sums[...] + mixed(last, ra[at(last)])).astype(BF)
 
     with mark("sends"):
-        for copy in g_copies:
-            copy.wait_send()
-        for k in [(k, k) for k in range(n)]:
-            f_copy(k).wait_send()
-            d_copy(k, c).wait_send()
-            e_copy(k, c).wait_send()
-            y_copy(k).wait_send()
-            if k != own:
-                a_copy(k).wait_send()
-            if k[0] >= NEAR:
-                z_copy(k).wait_send()
-                r_copy(k).wait_send()
-            elif k != own:
-                h_copy(k).wait_send()
-        x_copy.wait_send()
+        mine, other = xs.at[:, c, x], xs.at[:, c, 1 - x]
+        for ref, sem in (
+            (send_a.at[pl.ds(1, n - 1)], a_send), (mine, f_send), (mine, d_send), (other, e_send),
+            (ys, y_send), (zs.at[pl.ds(NEAR, n - NEAR)], z_send), (away_part, h_send),
+            (rs.at[pl.ds(NEAR, n - NEAR)], r_send), (ns.at[pl.ds(1, NEAR - 1)], n_send),
+            (gains.at[pl.ds(0, n_tp - 1)], g_send),
+        ):
+            remote(ref, ref, sem, h_recv, me, across).wait_send()
 
 
 def slot_pair(word):
@@ -497,15 +490,15 @@
             pltpu.VMEM((n, rows, cap), BF),
             pltpu.VMEM((n, rows, cap), BF),
             dma((4,)), dma((2 + n_tp,)),
-            dma((3,)), dma((3,)),
-            dma((n,)), dma((n,)),
-            dma((n,)), dma((n,)),
-            dma((n,)), dma((n,)),
-            dma((n,)), dma((n,)),
-            dma((n,)), dma((n,)),
-            dma((n,)), dma((n,)),
-            dma((n,)), dma((n,)),
-            dma, dma,
+            dma, dma((3,)),
+            dma, dma((n,)),
+            dma, dma((n,)),
+            dma, dma((n,)),
+            dma, dma((n,)),
+            dma, dma((n,)),
+            dma, dma((n,)),
+            dma, dma((n,)),
+            dma, dma, dma,
         ],
         compiler_params=pltpu.CompilerParams(
             collective_id=0, has_side_effects=True, vmem_limit_bytes=56 * 1024 * 1024

time: 58.7 us -> 58 us (0.988)
  Pallas kernels: 57.9 us -> 57 us
    pallas_call x1, Pallas kernels: 57.9 us -> 57 us  [routed(): pl.pallas_call(functools.partial(fused, n, n_tp), out_shape=pltpu.VMEM((r...]
where the time goes in v2:
time: 58 us; the launch traced here: 57.7 us
  Pallas kernels  57 us (98%)
  local copies, waits for them, and re-layouts  0.71 us (1%)
    pallas_call x1, Pallas kernels, routed(): pl.pallas_call(functools.partial(fused, n, n_tp), out_shape=pltpu.VMEM((r...  57 us

profile of v2, /device:TPU:8, one launch (start us, length us, event | category | flops | bytes accessed | tf_op | source)
XLA Modules:
  0.0 57.7 jit_solution(4633510049034741673)
XLA Ops:
  0.0 57.0 %shard_map.73 = bf16[256,512]{1,0:T(8,128)(2,1)S(1)} custom-call(bf16[256,512]{1,0:T(8,128)(2,1)} %tok_hbm.1, bf16[512]{0:T(512)(128)(2,1)} %gain_hbm.1, s32[2,256]{1,0:T(2,128)} %bitcast.2, f32[2,256]{1,0:T(2,128)} %bitcast.3, bf16[1,2048,1024]{2,1,0:T(8,128)(2,1)} %wg_hbm.1, bf16[1,2048,1024]{2,1,0:T(8,128)(2,1)} %wu_hbm.1, bf16[1,1024,2048]{2,1,0:T(8,128)(2,1)} %wd_hbm.1), custom_call_target="tpu_custom_call" | custom-call | tf_op jit(solution)/shard_map/pallas_call | solution.py:457
  57.0 0.7 %copy.9 = bf16[256,512]{1,0:T(8,128)(2,1)} copy(bf16[256,512]{1,0:T(8,128)(2,1)S(1)} %shard_map.73) | data formatting | bytes 524288

commit v3 on v2

--- a/solution.py
+++ b/solution.py
@@ -35,12 +35,12 @@
     "gu3:4/2", ">pass:3", "away:4/2", "here:4/2", "<give:6", "<take:5",
     "ready:3", "norm:3", "gu0:3", "<pair:4", ">home:2", ">give:6", "gu1:3", "gu2:3", "gu3:3",
     ">pass:7", "away:3", "here:3", "<pass:7",
-    "ready:7", "norm:7", "gu0:7", "pair:3", "gu1:7", "gu2:7", "gu3:7", "pass:5", "<give:4",
-    "away:7", "here:7",
+    "ready:7", "norm:7", "gu0:7", "<pair:3", "]pair:3", "gu1:7", "gu2:7", "gu3:7", "pass:5",
+    "<give:4", "away:7", "here:7",
     "ready:5", "norm:5", "gu0:5", "pair:7", ">give:4", "gu1:5", "gu2:5", "gu3:5", "away:5",
-    ">give:3", "here:5",
-    "pair:5", "<give:3", "give:7", "collect:1", "collect:2", "swap:0", "give:5", "gather:0",
-    "mix:6", "mix:4", "mix:3", "mix:7",
+    "]give:3", "here:5",
+    "pair:5", "[pair:3", "<give:3", "give:7", "collect:1", "collect:2", "swap:0", "give:5",
+    "[give:3", "gather:0", "mix:6", "mix:4", "mix:3", "mix:7",
 )
 
 
@@ -398,13 +398,17 @@
         for load in loads:
             load.wait()
 
-    def only(role, action):
+    def only(where, action):
         def run(k):
-            @pl.when(outer == role)
+            @pl.when(where)
             def _():
                 action(k)
         return run
 
+    places = {
+        "<": outer == 1, ">": outer == 0, "{": outer + high == 2, "}": outer - high == 1,
+        "[": outer - high == -1, "]": outer + high == 0,
+    }
     todo = {
         "take": take, "pass": pass_on, "ready": ready, "norm": normalize, "load": weights,
         "away": down_away, "here": down_here, "pair": pair, "give": give,
@@ -415,11 +419,9 @@
     for word in ORDER:
         name, ks = word.split(":")
         k = slot_pair(ks)
-        action = todo[name.strip("<>")]
-        if name[0] == "<":
-            action = only(1, action)
-        elif name[0] == ">":
-            action = only(0, action)
+        action = todo[name.strip("<>{}[]")]
+        if name[0] in places:
+            action = only(places[name[0]], action)
         with mark("%s_%s" % (name, ks.replace("/", "i"))):
             action(k)
 

time: 58 us -> 57.1 us (0.984)
  Pallas kernels: 57 us -> 55.7 us
    pallas_call x1, Pallas kernels: 57 us -> 55.7 us  [routed(): pl.pallas_call(functools.partial(fused, n, n_tp), out_shape=pltpu.VMEM((r...]
where the time goes in v3:
time: 57.1 us; the launch traced here: 56.4 us
  Pallas kernels  55.7 us (98%)
  local copies, waits for them, and re-layouts  0.71 us (1%)
    pallas_call x1, Pallas kernels, routed(): pl.pallas_call(functools.partial(fused, n, n_tp), out_shape=pltpu.VMEM((r...  55.7 us

profile of v3, /device:TPU:8, one launch (start us, length us, event | category | flops | bytes accessed | tf_op | source)
XLA Modules:
  0.0 56.4 jit_solution(13860606227478027908)
XLA Ops:
  0.0 55.7 %shard_map.73 = bf16[256,512]{1,0:T(8,128)(2,1)S(1)} custom-call(bf16[256,512]{1,0:T(8,128)(2,1)} %tok_hbm.1, bf16[512]{0:T(512)(128)(2,1)} %gain_hbm.1, s32[2,256]{1,0:T(2,128)} %bitcast.2, f32[2,256]{1,0:T(2,128)} %bitcast.3, bf16[1,2048,1024]{2,1,0:T(8,128)(2,1)} %wg_hbm.1, bf16[1,2048,1024]{2,1,0:T(8,128)(2,1)} %wu_hbm.1, bf16[1,1024,2048]{2,1,0:T(8,128)(2,1)} %wd_hbm.1), custom_call_target="tpu_custom_call" | custom-call | tf_op jit(solution)/shard_map/pallas_call | solution.py:459
  55.7 0.7 %copy.9 = bf16[256,512]{1,0:T(8,128)(2,1)} copy(bf16[256,512]{1,0:T(8,128)(2,1)S(1)} %shard_map.73) | data formatting | bytes 524288

commit v4 on v3

--- a/solution.py
+++ b/solution.py
@@ -93,7 +93,7 @@
     tok, gain, ids, share, wg, wu, wd, gains, slot_row, share_row, send_a, xs, block,
     hid, own_y, ys, yd, za, zs, zx, rs, ra, ns, na, away_part, far_part, sums, mix_hi, mix_lo,
     in_sem, w_sem, g_send, g_recv, a_send, a_recv,
-    f_send, f_recv, d_send, d_recv, e_send, e_recv, y_send, y_recv, z_send, z_recv, r_send, r_recv,
+    f_send, f_recv, d_send, d_recv, e_send, e_recv, y_send, z_send, r_send, r_recv,
     h_send, h_recv, n_send,
 ):
     me = lax.axis_index("ep")
@@ -266,11 +266,11 @@
 
     def y_copy(k):
         s = at(k)
-        return remote(ys.at[s], yd.at[s], y_send, y_recv.at[s], me, partner)
+        return remote(ys.at[s], yd.at[s], y_send, f_recv.at[s], me, partner)
 
     def z_copy(k):
         s = at(k)
-        return remote(zs.at[s], zx.at[s], z_send, z_recv.at[s], me, across)
+        return remote(zs.at[s], zx.at[s], z_send, a_recv.at[s], me, across)
 
     def h_copy(k):
         s = at(k)
@@ -497,8 +497,8 @@
             dma, dma((n,)),
             dma, dma((n,)),
             dma, dma((n,)),
-            dma, dma((n,)),
-            dma, dma((n,)),
+            dma,
+            dma,
             dma, dma((n,)),
             dma, dma, dma,
         ],

time: 57.1 us -> 57 us (level)
  no operation moved by 1% of the time
where the time goes in v4:
time: 57 us; the launch traced here: 56.3 us
  Pallas kernels  55.6 us (98%)
  local copies, waits for them, and re-layouts  0.71 us (1%)
    pallas_call x1, Pallas kernels, routed(): pl.pallas_call(functools.partial(fused, n, n_tp), out_shape=pltpu.VMEM((r...  55.6 us

profile of v4, /device:TPU:8, one launch (start us, length us, event | category | flops | bytes accessed | tf_op | source)
XLA Modules:
  0.0 56.3 jit_solution(8496010836305974920)
XLA Ops:
  0.0 55.6 %shard_map.73 = bf16[256,512]{1,0:T(8,128)(2,1)S(1)} custom-call(bf16[256,512]{1,0:T(8,128)(2,1)} %tok_hbm.1, bf16[512]{0:T(512)(128)(2,1)} %gain_hbm.1, s32[2,256]{1,0:T(2,128)} %bitcast.2, f32[2,256]{1,0:T(2,128)} %bitcast.3, bf16[1,2048,1024]{2,1,0:T(8,128)(2,1)} %wg_hbm.1, bf16[1,2048,1024]{2,1,0:T(8,128)(2,1)} %wu_hbm.1, bf16[1,1024,2048]{2,1,0:T(8,128)(2,1)} %wd_hbm.1), custom_call_target="tpu_custom_call" | custom-call | tf_op jit(solution)/shard_map/pallas_call | solution.py:459
  55.6 0.7 %copy.9 = bf16[256,512]{1,0:T(8,128)(2,1)} copy(bf16[256,512]{1,0:T(8,128)(2,1)S(1)} %shard_map.73) | data formatting | bytes 524288
